TPU v7x, 32 devices: a whole 2x2x4 slice. The times are simulated.
32 devices in a mesh: ep: 8 (over z, x), tp: 4 (over y, core).
Axes of the slice: x: 2, y: 2, z: 4, core: 2. Of those that a mesh axis runs over, the one named last changes fastest.
Arguments:
- tokens: bfloat16 [1024, 2048], P('ep'), may hold values from -6 to 6
- routes: int32 [1024, 2], P('ep'), may hold values from 0 to 7, all different within a row; in each aligned block of 128 rows (0 to 127, 128 to 255, ...) at most 36 rows name the same one
- route_gates: float32 [1024, 2], P('ep'), may hold values from 0.1 to 2
- cotangent: bfloat16 [1024, 2048], P('ep'), may hold values from -40 to 40
- w_gate: bfloat16 [8, 2048, 1536], P('ep', None, 'tp'), may hold values from -0.125 to 0.125
- w_up: bfloat16 [8, 2048, 1536], P('ep', None, 'tp'), may hold values from -0.125 to 0.125
- w_down: bfloat16 [8, 1536, 2048], P('ep', 'tp'), may hold values from -0.15625 to 0.15625
- s_gate: bfloat16 [2048, 1536], P(None, 'tp'), may hold values from -0.125 to 0.125
- s_up: bfloat16 [2048, 1536], P(None, 'tp'), may hold values from -0.125 to 0.125
- s_down: bfloat16 [1536, 2048], P('tp'), may hold values from -0.15625 to 0.15625
Outputs:
- token_grad: bfloat16 [1024, 2048], P('ep', 'tp')
- gate_grad: float32 [1024, 2], P('ep')
- grad_gate: float32 [8, 2048, 1536], P('ep', None, 'tp')
- grad_up: float32 [8, 2048, 1536], P('ep', None, 'tp')
- grad_down: float32 [8, 1536, 2048], P('ep', 'tp')
- grad_shared: float32 [1536, 2048], P(('tp', 'ep'))
- norm_in: float32 [8, 2, 2048], P('ep')
- norm_down: float32 [8, 1536], P('ep', 'tp')
- norm_shared: float32 [1536], P(('tp', 'ep'))
Inputs may be any that keep to these rules, and one draw needn't show every extreme that they name: `routes`: within the rows of one index of ep no expert is named by more than 36 assignments, a bound that some block reaches.
All inputs are finite; a program needn't handle non-finite values.
Results may differ from a plain program's by a relative error of at most 0.0095.
Values may be sent and summed in bfloat16 or wider, within the bound.
A program may use at most 64 MiB of HBM per device.

v0:
```python
import jax
import jax.numpy as jnp
from jax import lax
from jax.sharding import PartitionSpec as P


def swiglu_back(rows_x, rows_c, gate_weight, up_weight, down_weight):
    pre_gate = jnp.dot(rows_x, gate_weight, preferred_element_type=jnp.float32)
    pre_up = jnp.dot(rows_x, up_weight, preferred_element_type=jnp.float32)
    sigmoid_gate = jax.nn.sigmoid(pre_gate)
    activated = pre_gate * sigmoid_gate
    hidden = (activated * pre_up).astype(jnp.bfloat16)
    hidden_grad = jnp.einsum("rd,fd->rf", rows_c, down_weight, preferred_element_type=jnp.float32)
    d_gate = (hidden_grad * pre_up * sigmoid_gate * (1.0 + pre_gate * (1.0 - sigmoid_gate))).astype(
        jnp.bfloat16
    )
    d_up = (hidden_grad * activated).astype(jnp.bfloat16)
    joined_grad = jnp.concatenate([d_gate, d_up], axis=1)
    joined_weight = jnp.concatenate([gate_weight, up_weight], axis=1)
    back_rows = jnp.einsum(
        "rf,df->rd", joined_grad, joined_weight, preferred_element_type=jnp.float32
    )
    return (hidden, hidden_grad, d_gate, d_up, back_rows.astype(jnp.bfloat16))


def reduce_shared(shared_term):
    return lax.psum_scatter(shared_term, "ep", scatter_dimension=0, tiled=True)


def on_device(tokens, routes, route_gates, cotangent, w_gate, w_up, w_down, s_gate, s_up, s_down):
    ep_count = lax.axis_size("ep")
    tp_count = lax.axis_size("tp")
    tok_count, model_width = tokens.shape
    top_count = routes.shape[1]
    capacity = max(2, (9 * tok_count * top_count + 8 * ep_count - 1) // (8 * ep_count))
    feature_share = model_width // tp_count
    s_hidden, s_hidden_grad, s_d_gate, s_d_up, shared_piece = swiglu_back(
        tokens, cotangent, s_gate, s_up, s_down
    )
    shared_term = jnp.einsum("ts,td->sd", s_hidden, cotangent, preferred_element_type=jnp.float32)
    chosen = routes.reshape(tok_count * top_count)
    expert_ids = jnp.arange(ep_count, dtype=jnp.int32)
    one_hot = (chosen[:, None] == expert_ids[None, :]).astype(jnp.int32)
    ranks = jnp.sum((jnp.cumsum(one_hot, axis=0) - one_hot) * one_hot, axis=1)
    slot_of = chosen * capacity + ranks
    token_of = jnp.arange(tok_count * top_count, dtype=jnp.int32) // top_count
    row_token = jnp.full((ep_count * capacity,), tok_count, jnp.int32).at[slot_of].set(token_of)
    row_gate = (
        jnp.zeros((ep_count * capacity,), jnp.float32)
        .at[slot_of]
        .set(route_gates.reshape(tok_count * top_count))
    )
    padded_x = jnp.concatenate([tokens, jnp.zeros((1, model_width), jnp.bfloat16)], axis=0)
    padded_c = jnp.concatenate([cotangent, jnp.zeros((1, model_width), jnp.bfloat16)], axis=0)
    send_x = padded_x[row_token].reshape(ep_count, capacity, model_width)
    send_c = (row_gate[:, None] * padded_c[row_token].astype(jnp.float32)).astype(jnp.bfloat16)
    send_c = send_c.reshape(ep_count, capacity, model_width)
    start = lax.axis_index("tp") * feature_share
    part_x = lax.dynamic_slice_in_dim(send_x, start, feature_share, 2)
    part_c = lax.dynamic_slice_in_dim(send_c, start, feature_share, 2)
    moved_x, moved_c = (
        lax.all_to_all(part_x, "ep", split_axis=0, concat_axis=0, tiled=True),
        lax.all_to_all(part_c, "ep", split_axis=0, concat_axis=0, tiled=True),
    )
    recv_x, recv_c = (
        lax.all_gather(moved_x, "tp", axis=2, tiled=True),
        lax.all_gather(moved_c, "tp", axis=2, tiled=True),
    )
    rows_x = recv_x.reshape(ep_count * capacity, model_width)
    rows_c = recv_c.reshape(ep_count * capacity, model_width)
    hidden, hidden_grad, d_gate, d_up, slot_part = swiglu_back(
        rows_x, rows_c, w_gate[0], w_up[0], w_down[0]
    )
    gate_part = jnp.sum(hidden.astype(jnp.float32) * hidden_grad, axis=1)
    g_gate = jnp.einsum("rd,rf->df", rows_x, d_gate, preferred_element_type=jnp.float32)
    g_up = jnp.einsum("rd,rf->df", rows_x, d_up, preferred_element_type=jnp.float32)
    g_down = jnp.einsum("rf,rd->fd", hidden, rows_c, preferred_element_type=jnp.float32)
    square_part = jnp.stack([jnp.sum(g_gate**2, axis=1), jnp.sum(g_up**2, axis=1)], axis=0)
    gate_total, square_total = lax.psum((gate_part, square_part), "tp")
    ff_total = tp_count * w_gate.shape[2]
    norm_in = (square_total / ff_total)[None]
    gate_rounded = gate_total.astype(jnp.bfloat16)
    back_rows, back_dots = (
        lax.all_to_all(
            slot_part.reshape(ep_count, capacity, model_width),
            "ep",
            split_axis=0,
            concat_axis=0,
            tiled=True,
        ),
        lax.all_to_all(
            gate_rounded.reshape(ep_count, capacity), "ep", split_axis=0, concat_axis=0, tiled=True
        ),
    )
    picked = back_rows.reshape(ep_count * capacity, model_width)[slot_of].reshape(
        tok_count, top_count, model_width
    )
    partial_value = jnp.sum(picked.astype(jnp.float32), axis=1) + shared_piece.astype(jnp.float32)
    token_parts = lax.all_to_all(partial_value[None], "tp", split_axis=2, concat_axis=0, tiled=True)
    token_grad = jnp.sum(token_parts, axis=0).astype(jnp.bfloat16)
    gate_grad = (
        back_dots.reshape(ep_count * capacity)[slot_of]
        .reshape(tok_count, top_count)
        .astype(jnp.float32)
        / route_gates
    )
    grad_shared = reduce_shared(shared_term)
    norm_shared = jnp.mean(grad_shared**2, axis=1)
    norm_down = jnp.mean(g_down**2, axis=1)[None]
    return (
        token_grad,
        gate_grad,
        g_gate[None],
        g_up[None],
        g_down[None],
        grad_shared,
        norm_in,
        norm_down,
        norm_shared,
    )


def solution(mesh):
    placed = (
        P("ep", None),
        P("ep", None),
        P("ep", None),
        P("ep", None),
        P("ep", None, "tp"),
        P("ep", None, "tp"),
        P("ep", "tp", None),
        P(None, "tp"),
        P(None, "tp"),
        P("tp", None),
    )
    return jax.shard_map(
        on_device,
        mesh=mesh,
        in_specs=placed,
        out_specs=(
            P("ep", "tp"),
            P("ep", None),
            P("ep", None, "tp"),
            P("ep", None, "tp"),
            P("ep", "tp", None),
            P(("tp", "ep"), None),
            P("ep", None, None),
            P("ep", "tp"),
            P(("tp", "ep")),
        ),
        check_vma=False,
    )
```

profile of v0, /device:TPU:0, one launch (start us, length us, event | category | flops | bytes accessed | tf_op | source)
XLA Modules:
  0.0 180.7 jit_solution(10652360249780114024)
XLA Ops:
  13.7 2.4 %gather_fusion = bf16[288,2048]{1,0:T(8,128)(2,1)S(1)} fusion(bf16[129,2048]{1,0:T(8,128)(2,1)S(1)} %concatenate.18, s32[1024]{0:T(1024)S(1)} %pad_clamp_fusion.1), kind=kCustom, calls=%fused_computation | custom fusion | bytes 2360448 | tf_op jit(solution)/shard_map/gather | solution.py:56
  20.7 18.1 %all_to_all.37 = bf16[8,36,512]{2,1,0:T(8,128)(2,1)} all-to-all(bf16[8,36,512]{2,1,0:T(8,128)(2,1)S(1)} %fusion.25), channel_id=1, replica_groups=mesh['ep'=8,'tp'=4] {'ep'}, dimensions={0} | all-to-all | bytes 589824 | tf_op jit(solution)/shard_map/all_to_all | solution.py:63
  38.9 2.4 %gather_fusion.1 = bf16[288,2048]{1,0:T(8,128)(2,1)S(1)} fusion(bf16[129,2048]{1,0:T(8,128)(2,1)S(1)} %concatenate.19, s32[1024]{0:T(1024)S(1)} %pad_clamp_fusion.1), kind=kCustom, calls=%fused_computation.1 | custom fusion | bytes 2360448 | tf_op jit(solution)/shard_map/gather | solution.py:55
  43.6 13.9 %all_to_all.38 = bf16[8,36,512]{2,1,0:T(8,128)(2,1)} all-to-all(bf16[8,36,512]{2,1,0:T(8,128)(2,1)S(1)} %constant_dynamic-slice_fusion), channel_id=1, replica_groups=mesh['ep'=8,'tp'=4] {'ep'}, dimensions={0} | all-to-all | bytes 589824 | tf_op jit(solution)/shard_map/all_to_all | solution.py:62
  62.1 2.3 %fusion.34 = f32[384,2048]{1,0:T(8,128)} fusion(bf16[128,2048]{1,0:T(8,128)(2,1)S(1)} %copy-done.3, f32[128,384]{1,0:T(8,128)S(1)} %fusion.51, f32[128,384]{1,0:T(8,128)S(1)} %get-tuple-element.53), kind=kOutput, calls=%fused_computation.44 | convolution fusion | flops 201621504 | bytes 4063232 | tf_op jit(solution)/shard_map/ts,td->sd/dot_general | solution.py:40
  64.5 2.3 %reshape.118 = bf16[288,2048]{1,0:T(8,128)(2,1)} reshape(bf16[8,36,2048]{2,1,0:T(8,128)(2,1)} %all-gather.3.cloned.1.call-done) | data formatting | bytes 2359296 | tf_op jit(solution)/shard_map/reshape | solution.py:70
  66.7 8.6 %all-gather.5.cloned.1.call-done = bf16[8,36,2048]{2,1,0:T(8,128)(2,1)} async-done(((bf16[8,36,512]{2,1,0:T(8,128)(2,1)}), bf16[8,36,2048]{2,1,0:T(8,128)(2,1)}) %all-gather.5.cloned.1.call-update) | async-done | bytes 1179664 | tf_op jit(solution)/shard_map/all_gather | solution.py:66
  76.8 2.3 %fusion.45 = f32[288,384]{1,0:T(8,128)S(1)} fusion(bf16[288,2048]{1,0:T(8,128)(2,1)S(1)} %reshape.120, bf16[1,2048,384]{2,1,0:T(8,128)(2,1)} %param.14), kind=kOutput, calls=%fused_computation.72 | convolution fusion | flops 452984832 | bytes 3194880 | tf_op jit(solution)/shard_map/dot_general | solution.py:8
  84.2 2.3 %reshape.121 = bf16[8,36,2048]{2,1,0:T(8,128)(2,1)} reshape(bf16[288,2048]{1,0:T(8,128)(2,1)} %fusion.8) | data formatting | bytes 2359296 | tf_op jit(solution)/shard_map/reshape | solution.py:85
  86.4 5.5 %all-to-all-start.2 = ((bf16[8,36,2048]{2,1,0:T(8,128)(2,1)}), bf16[8,36,2048]{2,1,0:T(8,128)(2,1)}, u32[]{:S(2)}, u32[]{:S(2)}) async-start(bf16[8,36,2048]{2,1,0:T(8,128)(2,1)} %reshape.121), calls=%async_computation.2 | async-start | bytes 2621440 | tf_op jit(solution)/shard_map/all_to_all | solution.py:84
  91.9 2.7 %multiply_reduce_fusion.2 = (f32[2048]{0:T(1024)S(1)}, f32[2048,384]{0,1:T(8,128)}) fusion(bf16[288,2048]{1,0:T(8,128)(2,1)S(1)} %reshape.120, bf16[288,384]{1,0:T(8,128)(2,1)S(1)} %get-tuple-element.49), kind=kOutput, calls=%fused_computation.16 | convolution fusion | flops 454555648 | bytes 4554752 | tf_op jit(solution)/shard_map/rd,rf->df/dot_general | solution.py:75
  94.6 2.7 %multiply_reduce_fusion.1 = (f32[2048]{0:T(1024)S(1)}, f32[2048,384]{0,1:T(8,128)}) fusion(bf16[288,2048]{1,0:T(8,128)(2,1)S(1)} %reshape.120, bf16[288,384]{1,0:T(8,128)(2,1)S(1)} %get-tuple-element.50), kind=kOutput, calls=%fused_computation.15 | convolution fusion | flops 454555648 | bytes 4554752 | tf_op jit(solution)/shard_map/rd,rf->df/dot_general | solution.py:76
  97.4 11.1 %all-reduce.2 = (bf16[288]{0:T(512)(128)(2,1)S(1)}, f32[2,2048]{1,0:T(2,128)S(1)}) all-reduce(f32[288]{0:T(512)S(1)} %get-tuple-element.47, f32[2,2048]{1,0:T(2,128)S(1)} %pad_maximum_fusion), channel_id=1, replica_groups=mesh['ep'=8,'tp'=4] {'tp'}, use_global_device_ids=true, to_apply=%region_8.9 | all-reduce | flops 4384 | bytes 34496 | tf_op jit(solution)/shard_map/psum | solution.py:79
  109.1 17.8 %all-to-all-done.2 = bf16[8,36,2048]{2,1,0:T(8,128)(2,1)} async-done(((bf16[8,36,2048]{2,1,0:T(8,128)(2,1)}), bf16[8,36,2048]{2,1,0:T(8,128)(2,1)}, u32[]{:S(2)}, u32[]{:S(2)}) %all-to-all-start.2) | async-done | bytes 1179680 | tf_op jit(solution)/shard_map/all_to_all | solution.py:84
  126.9 3.9 %all-to-all-start.4 = ((bf16[8,1,36]{2,1,0:T(2,128)(2,1)}), bf16[8,1,36]{2,1,0:T(2,128)(2,1)S(1)}, u32[]{:S(2)}, u32[]{:S(2)}) async-start(bf16[8,1,36]{2,1,0:T(2,128)(2,1)} %all_to_all.31), calls=%async_computation.4 | async-start | bytes 8192 | tf_op jit(solution)/shard_map/all_to_all | solution.py:91
  132.2 2.4 %gather_fusion.2 = bf16[256,2048]{1,0:T(8,128)(2,1)} fusion(bf16[288,2048]{1,0:T(8,128)(2,1)S(1)} %reshape.122, s32[1024]{0:T(1024)S(1)} %pad_clamp_fusion), kind=kCustom, calls=%fused_computation.2 | custom fusion | bytes 2098176 | tf_op jit(solution)/shard_map/gather | solution.py:95
  134.6 3.3 %reshape.125 = f32[128,2,2048]{2,1,0:T(2,128)} reshape(bf16[256,2048]{1,0:T(8,128)(2,1)} %gather_fusion.2) | data formatting | bytes 3145728 | tf_op jit(solution)/shard_map/convert_element_type | solution.py:98
  137.9 5.2 %reduce_sum.76 = f32[128,2048]{1,0:T(8,128)} reduce(f32[128,2,2048]{2,1,0:T(2,128)} %reshape.125, f32[]{:T(128)} %constant.17.clone.1), dimensions={1}, to_apply=%region_5.6 | reduce | flops 262144 | bytes 3145732 | tf_op jit(solution)/shard_map/reduce_sum | solution.py:98
  143.2 3.9 %fusion.20 = f32[1,128,2048]{2,1,0:T(8,128)} fusion(f32[128,2048]{1,0:T(8,128)} %reduce_sum.76, bf16[2048,384]{1,0:T(8,128)(2,1)S(1)} %copy-done.7, bf16[2048,384]{1,0:T(8,128)(2,1)} %param.17, bf16[128,384]{1,0:T(8,128)(2,1)} %get-tuple-element.52, bf16[128,384]{1,0:T(8,128)(2,1)S(1)} %get-tuple-element.51), kind=kOutput, calls=%fused_computation.21 | convolution fusion | flops 410124288 | bytes 5439488 | tf_op jit(solution)/shard_map/rf,df->rd/dot_general | solution.py:20
  147.0 3.6 %copy.43 = f32[1,128,2048]{1,0,2:T(1,128)} copy(f32[1,128,2048]{2,1,0:T(8,128)} %fusion.20) | data formatting | bytes 2097152 | tf_op jit(solution)/shard_map/broadcast_in_dim | solution.py:99
  150.7 4.4 %all-to-all-start.3 = ((f32[1,128,2048]{1,0,2:T(1,128)}), f32[1,128,2048]{1,0,2:T(1,128)}, u32[]{:S(2)}, u32[]{:S(2)}) async-start(f32[1,128,2048]{1,0,2:T(1,128)} %copy.43), calls=%async_computation.3 | async-start | bytes 2097152 | tf_op jit(solution)/shard_map/all_to_all | solution.py:99
  155.1 2.7 %multiply_reduce_fusion = (f32[384]{0:T(512)S(1)}, f32[384,2048]{1,0:T(8,128)}) fusion(bf16[288,384]{1,0:T(8,128)(2,1)S(1)} %copy-done.8, bf16[288,2048]{1,0:T(8,128)(2,1)S(1)} %copy-done.2), kind=kOutput, calls=%fused_computation.14 | convolution fusion | flops 454557312 | bytes 4548096 | tf_op jit(solution)/shard_map/rf,rd->fd/dot_general | solution.py:77
  158.3 3.5 %copy.48 = f32[1,2048,384]{2,1,0:T(8,128)} copy(f32[1,2048,384]{1,2,0:T(8,128)} %bitcast.47) | data formatting | bytes 6291456
  161.9 3.5 %copy.49 = f32[1,2048,384]{2,1,0:T(8,128)} copy(f32[1,2048,384]{1,2,0:T(8,128)} %bitcast.48) | data formatting | bytes 6291456
  (87 shorter events, 34.1 us)
Async XLA Ops:
  8.0 71.9 %copy-start = (bf16[1,384,2048]{2,1,0:T(8,128)(2,1)S(1)}, bf16[1,384,2048]{2,1,0:T(8,128)(2,1)}, u32[]{:S(2)}) copy-start(bf16[1,384,2048]{2,1,0:T(8,128)(2,1)} %param.16) | copy-start | bytes 4718596
  8.0 56.4 %all-gather.3.cloned.1.call-start = ((), (), s32[]{:S(2)}) async-start(), calls=%async_computation.6 | async-start | bytes 1638400 | tf_op jit(solution)/shard_map/all_gather | solution.py:67
  16.1 1.6 copy-start.9
  17.7 21.1 %copy-start.4 = (bf16[128,2048]{1,0:T(8,128)(2,1)S(1)}, bf16[128,2048]{1,0:T(8,128)(2,1)}, u32[]{:S(2)}) copy-start(bf16[128,2048]{1,0:T(8,128)(2,1)} %param.10) | copy-start | bytes 1572868
  38.8 36.5 %all-gather.5.cloned.1.call-start = ((), (), s32[]{:S(2)}) async-start(), calls=%async_computation.7 | async-start | bytes 1638400 | tf_op jit(solution)/shard_map/all_gather | solution.py:66
  42.6 15.0 %copy-start.5 = (bf16[128,2048]{1,0:T(8,128)(2,1)S(1)}, bf16[128,2048]{1,0:T(8,128)(2,1)}, u32[]{:S(2)}) copy-start(bf16[128,2048]{1,0:T(8,128)(2,1)} %param.10) | copy-start | bytes 1572868
  43.6 15.9 %copy-start.3 = (bf16[128,2048]{1,0:T(8,128)(2,1)S(1)}, bf16[128,2048]{1,0:T(8,128)(2,1)}, u32[]{:S(2)}) copy-start(bf16[128,2048]{1,0:T(8,128)(2,1)} %param.13) | copy-start | bytes 1572868
  57.5 114.1 %reduce-scatter.2.cloned.1.call-start = ((), (), s32[]{:S(2)}) async-start(), calls=%async_computation.8 | async-start | bytes 3538944 | tf_op jit(solution)/shard_map/reduce_scatter | solution.py:27
  57.6 2.0 %copy-start.6 = (bf16[384,2048]{1,0:T(8,128)(2,1)S(1)}, bf16[384,2048]{1,0:T(8,128)(2,1)}, u32[]{:S(2)}) copy-start(bf16[384,2048]{1,0:T(8,128)(2,1)} %param.19) | copy-start | bytes 4718596
  59.6 1.4 copy-start.12
  76.8 2.3 %copy-start.10 = (bf16[1,2048,384]{2,1,0:T(8,128)(2,1)S(1)}, bf16[1,2048,384]{2,1,0:T(8,128)(2,1)}, u32[]{:S(2)}) copy-start(bf16[1,2048,384]{2,1,0:T(8,128)(2,1)} %param.15) | copy-start | bytes 4718596
  79.1 1.3 copy-start.1
  80.4 1.6 copy-start.11
  86.4 40.5 %all-to-all-start.2 = ((bf16[8,36,2048]{2,1,0:T(8,128)(2,1)}), bf16[8,36,2048]{2,1,0:T(8,128)(2,1)}, u32[]{:S(2)}, u32[]{:S(2)}) async-start(bf16[8,36,2048]{2,1,0:T(8,128)(2,1)} %reshape.121), calls=%async_computation.2 | async-start | bytes 2621440 | tf_op jit(solution)/shard_map/all_to_all | solution.py:84
  126.9 23.7 %all-to-all-start.4 = ((bf16[8,1,36]{2,1,0:T(2,128)(2,1)}), bf16[8,1,36]{2,1,0:T(2,128)(2,1)S(1)}, u32[]{:S(2)}, u32[]{:S(2)}) async-start(bf16[8,1,36]{2,1,0:T(2,128)(2,1)} %all_to_all.31), calls=%async_computation.4 | async-start | bytes 8192 | tf_op jit(solution)/shard_map/all_to_all | solution.py:91
  137.9 5.2 %copy-start.7 = (bf16[2048,384]{1,0:T(8,128)(2,1)S(1)}, bf16[2048,384]{1,0:T(8,128)(2,1)}, u32[]{:S(2)}) copy-start(bf16[2048,384]{1,0:T(8,128)(2,1)} %param.18) | copy-start | bytes 4718596
  150.6 4.4 %copy-start.2 = (bf16[288,2048]{1,0:T(8,128)(2,1)S(1)}, bf16[288,2048]{1,0:T(8,128)(2,1)}, u32[]{:S(2)}) copy-start(bf16[288,2048]{1,0:T(8,128)(2,1)} %reshape.118) | copy-start | bytes 3538948
  150.7 4.4 %copy-start.8 = (bf16[288,384]{1,0:T(8,128)(2,1)S(1)}, bf16[288,384]{1,0:T(8,128)(2,1)}, u32[]{:S(2)}) copy-start(bf16[288,384]{1,0:T(8,128)(2,1)} %get-tuple-element.48) | copy-start | bytes 663556
  150.7 18.9 %all-to-all-start.3 = ((f32[1,128,2048]{1,0,2:T(1,128)}), f32[1,128,2048]{1,0,2:T(1,128)}, u32[]{:S(2)}, u32[]{:S(2)}) async-start(f32[1,128,2048]{1,0,2:T(1,128)} %copy.43), calls=%async_computation.3 | async-start | bytes 2097152 | tf_op jit(solution)/shard_map/all_to_all | solution.py:99
Sparse Core Ops, SparseCore 0:
  38.9 16.6 all-gather.2
  57.6 17.6 all-gather.4
Sparse Core Ops, SparseCore 1:
  64.5 89.7 reduce-scatter.1
where the time goes:
time: 182 us; the launch traced here: 181 us
  local copies, waits for them, and re-layouts  44.5 us (24%)
  blocking collectives  43 us (24%)
  waiting for transfers between devices  27.1 us (15%)
  matrix products  24.8 us (14%)
  between operations  15.8 us (9%)
  starting transfers between devices  13.9 us (8%)
  other arithmetic  11.5 us (6%)
    all_to_all x1, blocking collectives, on_device(): lax.all_to_all(part_c, 'ep', split_axis=0, concat_axis=0, tiled=True)  18.1 us
    all_to_all x1, waiting for transfers between devices, on_device(): lax.all_to_all(slot_part.reshape(ep_count, capacity, model_width), 'ep',...  17.8 us
    all_to_all x1, blocking collectives, on_device(): lax.all_to_all(part_x, 'ep', split_axis=0, concat_axis=0, tiled=True)  13.9 us
    psum x1, blocking collectives, on_device(): gate_total, square_total = lax.psum((gate_part, square_part), 'tp')  11.1 us
    unnamed x32, local copies, waits for them, and re-layouts  10.8 us
    all_gather x1, waiting for transfers between devices, on_device(): lax.all_gather(moved_x, 'tp', axis=2, tiled=True)  8.61 us
    dot_general x2, matrix products, swiglu_back(): jnp.einsum('rf,df->rd', joined_grad, joined_weight, preferred_element_typ...  6.02 us
    all_to_all x1, starting transfers between devices, on_device(): lax.all_to_all(slot_part.reshape(ep_count, capacity, model_width), 'ep',...  5.52 us
  transfers between devices with their start and end apart: 6, of which 3 were waited for; matrix products, arithmetic and copies ran while one was open for 36% of the time, Pallas kernels for 0%

commit v1 on v0

v1 whole, which is shorter than its diff:
```python
import functools

import jax
import jax.numpy as jnp
from jax import lax
from jax.experimental import pallas as pl
from jax.experimental.pallas import tpu as pltpu
from jax.sharding import PartitionSpec as P

MESH = pl.DeviceIdType.MESH
CORES = 2
BF = jnp.bfloat16
F32 = jnp.float32


def dot(a, b, ca=1, cb=0):
    return lax.dot_general(a, b, (((ca,), (cb,)), ((), ())), preferred_element_type=F32)


def activations(pre_gate, pre_up, hidden_grad):
    sig = jax.nn.sigmoid(pre_gate)
    act = pre_gate * sig
    hidden = (act * pre_up).astype(BF)
    d_gate = (hidden_grad * pre_up * sig * (1.0 + pre_gate * (1.0 - sig))).astype(BF)
    d_up = (hidden_grad * act).astype(BF)
    return hidden, d_gate, d_up


def body(
    ep, tp, cap_pad,
    slot_row, slot_col, gates, tokens, cot, wg_h, wu_h, wd_h, sg_h, su_h, sd_h,
    token_out, gate_out, shared_out, norm_in_out, norm_down_out, norm_sh_out,
    x_out, c_out, hid_out, dg_out, du_out,
    wg, wu, wd, sg, su, sd, send, rx, acc, prod, term, term_rx,
    part_a, part_own, recv_a, part_b, recv_b, back_tx, back_rx, shared_tot,
    gpart, grecv, gsend, gback, sq, sq_rx,
    w_sem, out_sem, d1_s, d1_r, d2_s, d2_r, pass_s, rs_s, rs_r, ra_s, ra_r, rb_s, rb_r,
    bk_s, bk_r, g_s, g_r, gb_s, gb_r, q_s, q_r,
):
    me = lax.axis_index("ep")
    j = lax.axis_index("tp")
    core = lax.rem(j, CORES)
    y = lax.div(j, CORES)
    mate = j + 1 - 2 * core
    ny = tp // CORES
    rows = ep * cap_pad
    tok, width = tokens.shape
    share = width // tp
    top = slot_row.shape[0]
    ff = wg.shape[1]
    sr = shared_out.shape[0]

    loads = [
        pltpu.make_async_copy(src, dst, w_sem.at[n])
        for n, (src, dst) in enumerate(
            [(sg_h, sg), (su_h, su), (sd_h, sd), (wg_h, wg), (wu_h, wu), (wd_h, wd)]
        )
    ]
    for load in loads:
        load.start()

    def ep_peer(step):
        return lax.rem(me + step, ep)

    def remote(src, dst, ssem, rsem, **where):
        copy = pltpu.make_async_remote_copy(
            src_ref=src, dst_ref=dst, send_sem=ssem, recv_sem=rsem,
            device_id=where, device_id_type=MESH,
        )
        copy.start()
        return copy

    barrier = pltpu.get_barrier_semaphore()
    for step in range(1, ep):
        pl.semaphore_signal(barrier, inc=1, device_id={"ep": ep_peer(step)}, device_id_type=MESH)
    for step in range(1, tp):
        pl.semaphore_signal(
            barrier, inc=1, device_id={"tp": lax.rem(j + step, tp)}, device_id_type=MESH
        )

    cols = pl.ds(pl.multiple_of(j * share, share), share)
    x_share = tokens[:, cols]
    c_share = cot[:, cols].astype(F32)
    slot_ids = lax.broadcasted_iota(jnp.int32, (rows, tok), 0)
    any_hot = jnp.zeros((rows, tok), F32)
    c_rows = jnp.zeros((rows, share), F32)
    for k in range(top):
        hot = jnp.where(slot_ids == slot_row[k : k + 1, :], 1.0, 0.0)
        any_hot = any_hot + hot
        c_rows = c_rows + dot(hot.astype(BF), (gates[:, k : k + 1] * c_share).astype(BF))
    x_rows = dot(any_hot.astype(BF), x_share)
    send[0] = x_rows.astype(BF).reshape(ep, cap_pad, share)
    send[1] = c_rows.astype(BF).reshape(ep, cap_pad, share)

    pl.semaphore_wait(barrier, ep + tp - 2)

    waits = []
    for step in range(1, ep):
        to = ep_peer(step)
        waits.append(
            remote(send.at[:, to], rx.at[j, :, me], d1_s.at[step], d1_r.at[step], ep=to)
        )
    rx[j, :, me] = send[:, me]

    def forward(source):
        block = rx.at[j, :, source]
        remote(block, block, d2_s.at[0], d2_r.at[j], tp=mate)
        for step in range(1, ny):
            to = lax.rem(y + step, ny) * CORES + core
            remote(block, block, d2_s.at[step], d2_r.at[j], tp=to)

    forward(me)

    for load in loads[:3]:
        load.wait()
    s_hidden, s_dg, s_du = activations(
        dot(tokens[...], sg[...]), dot(tokens[...], su[...]), dot(cot[...], sd[...], 1, 1)
    )

    d1 = list(waits)
    for step in range(1, ep):
        d1[step - 1].wait_recv()
        forward(lax.rem(me - step + ep, ep))

    for chunk in range(tp):
        at = slice(chunk * share, (chunk + 1) * share)
        value = dot(s_hidden, cot[:, at], 0, 0)
        for i in range(ep):
            term[i, :, at] = value[i * sr : (i + 1) * sr].astype(BF)
    for step in range(1, ep):
        to = ep_peer(step)
        waits.append(remote(term.at[to], term_rx.at[me], rs_s.at[step], rs_r.at[step], ep=to))
    rs = waits[ep - 1 :]

    def part_of(block, d_gate, d_up, gate_w, up_w):
        at = pl.ds(pl.multiple_of(block * share, share), share)
        return dot(d_gate, gate_w[at, :], 1, 1) + dot(d_up, up_w[at, :], 1, 1)

    for yq in range(ny):
        part_a[yq, rows:, :] = part_of(yq * CORES + 1 - core, s_dg, s_du, sg, su).astype(BF)
        part_own[yq, rows:, :] = part_of(yq * CORES + core, s_dg, s_du, sg, su)

    for load in loads[3:]:
        load.wait()
    acc[...] = jnp.zeros_like(acc)

    def add_share(t):
        at = pl.ds(pl.multiple_of(t * share, share), share)
        x_in = rx[t, 0].reshape(rows, share)
        c_in = rx[t, 1].reshape(rows, share)
        acc[0] += dot(x_in, wg[at, :])
        acc[1] += dot(x_in, wu[at, :])
        acc[2] += dot(c_in, wd[:, at], 1, 1)

    def arrived(t):
        pltpu.make_async_remote_copy(
            src_ref=rx.at[t], dst_ref=rx.at[t], send_sem=d2_s.at[0], recv_sem=d2_r.at[t],
            device_id={"tp": mate}, device_id_type=MESH,
        ).wait_recv()

    add_share(j)
    passed = []
    for step in range(1, ny):
        t = lax.rem(y - step + ny, ny) * CORES + core
        arrived(t)
        passed.append(remote(rx.at[t], rx.at[t], pass_s.at[step], d2_r.at[tp + step], tp=mate))
        if step == 1:
            arrived(mate)
            add_share(mate)
        add_share(t)
    for step in range(1, ny):
        t = lax.rem(y - step + ny, ny) * CORES + 1 - core
        passed[step - 1].wait_recv()
        add_share(t)

    outs = []
    for t in range(tp):
        at = pl.ds(t * share, share)
        outs.append(pltpu.make_async_copy(rx.at[t, 0], x_out.at[:, :, at], out_sem.at[2 * t]))
        outs.append(pltpu.make_async_copy(rx.at[t, 1], c_out.at[:, :, at], out_sem.at[2 * t + 1]))
    for out in outs:
        out.start()

    hidden, d_gate, d_up = activations(acc[0], acc[1], acc[2])
    hid_out[...] = hidden
    dg_out[...] = d_gate
    du_out[...] = d_up
    prod[...] = hidden.astype(F32) * acc[2]

    ra = []
    for yq in range(ny):
        part_a[yq, :rows, :] = part_of(yq * CORES + 1 - core, d_gate, d_up, wg, wu).astype(BF)
        ra.append(remote(part_a.at[yq], recv_a.at[yq], ra_s.at[yq], ra_r.at[yq], tp=mate))
    for yq in range(ny):
        part_own[yq, :rows, :] = part_of(yq * CORES + core, d_gate, d_up, wg, wu)

    gpart[...] = jnp.zeros_like(gpart)
    ones = jnp.ones((8, ff), F32)
    for i in range(ep):
        gpart[i, :, :cap_pad] = lax.dot_general(
            ones, prod[i * cap_pad : (i + 1) * cap_pad, :], (((1,), (1,)), ((), ())),
            preferred_element_type=F32, precision=lax.Precision.HIGHEST,
        )
    gx = []
    for step in range(1, tp):
        gx.append(remote(gpart, grecv.at[step], g_s.at[step], g_r.at[step], tp=lax.rem(j + step, tp)))

    for copy in ra:
        copy.wait_recv()
    rb = []
    for step in range(1, ny):
        yq = lax.rem(y + step, ny)
        part_b[step] = (part_own[yq] + recv_a[yq].astype(F32)).astype(BF)
        rb.append(
            remote(part_b.at[step], recv_b.at[step], rb_s.at[step], rb_r.at[step], tp=yq * CORES + core)
        )

    norm_down = jnp.zeros((ff, 1), F32)
    for t in range(tp):
        at = slice(t * share, (t + 1) * share)
        x_in = rx[t, 0].reshape(rows, share)
        c_in = rx[t, 1].reshape(rows, share)
        sq[0:1, at] = jnp.sum(jnp.square(dot(dg_out[...], x_in, 0, 0)), axis=0, keepdims=True)
        sq[1:2, at] = jnp.sum(jnp.square(dot(du_out[...], x_in, 0, 0)), axis=0, keepdims=True)
        norm_down += jnp.sum(jnp.square(dot(hid_out[...], c_in, 0, 0)), axis=1, keepdims=True)
    norm_down_out[...] = norm_down / width
    qx = []
    for step in range(1, tp):
        qx.append(remote(sq, sq_rx.at[step], q_s.at[step], q_r.at[step], tp=lax.rem(j + step, tp)))

    for copy in gx:
        copy.wait_recv()
    total = gpart[...]
    for step in range(1, tp):
        total = total + grecv[step]
    gsend[...] = total.astype(BF).astype(F32)
    gb = []
    for step in range(1, ep):
        to = ep_peer(step)
        gb.append(remote(gsend.at[to], gback.at[me], gb_s.at[step], gb_r.at[step], ep=to))
    gback[me] = gsend[me]

    for copy in rb:
        copy.wait_recv()
    part = part_own[y] + recv_a[y].astype(F32)
    for step in range(1, ny):
        part = part + recv_b[step].astype(F32)
    back_tx[...] = part[:rows].astype(BF).reshape(ep, cap_pad, share)
    shared_tot[...] = part[rows:]
    bk = []
    for step in range(1, ep):
        to = ep_peer(step)
        bk.append(remote(back_tx.at[to], back_rx.at[me], bk_s.at[step], bk_r.at[step], ep=to))
    back_rx[me] = back_tx[me]

    for copy in qx:
        copy.wait_recv()
    squares = sq[...]
    for step in range(1, tp):
        squares = squares + sq_rx[step]
    norm_in_out[...] = squares / (tp * ff)

    for copy in rs:
        copy.wait_recv()
    term_rx[me] = term[me]
    grad = term_rx[0].astype(F32)
    for i in range(1, ep):
        grad = grad + term_rx[i].astype(F32)
    shared_out[...] = grad
    norm_sh_out[...] = jnp.mean(jnp.square(grad), axis=1, keepdims=True)

    for copy in gb:
        copy.wait_recv()
    lane = lax.broadcasted_iota(jnp.int32, (tok, 128), 1)
    for k in range(top):
        picked = jnp.zeros((tok, 128), F32)
        for i in range(ep):
            hit = (lane < cap_pad) & (slot_col[:, k : k + 1] == lane + i * cap_pad)
            picked = picked + jnp.where(hit, gback[i, 0:1, :], 0.0)
        gate_out[:, k : k + 1] = jnp.sum(picked, axis=1, keepdims=True) / gates[:, k : k + 1]

    place = lax.broadcasted_iota(jnp.int32, (tok, rows), 1)
    pick = jnp.zeros((tok, rows), F32)
    for k in range(top):
        pick = pick + jnp.where(place == slot_col[:, k : k + 1], 1.0, 0.0)
    for copy in bk:
        copy.wait_recv()
    token_out[...] = (
        dot(pick.astype(BF), back_rx[...].reshape(rows, share)) + shared_tot[...]
    ).astype(BF)

    for step in range(ny):
        pltpu.make_async_remote_copy(
            src_ref=rx.at[j], dst_ref=rx.at[j], send_sem=d2_s.at[step], recv_sem=d2_r.at[j],
            device_id={"tp": mate}, device_id_type=MESH,
        ).wait_send()
    for copy in waits + passed + ra + gx + rb + qx + gb + bk:
        copy.wait_send()
    for out in outs:
        out.wait()


def on_device(
    ep, tp, tokens, routes, route_gates, cotangent, w_gate, w_up, w_down, s_gate, s_up, s_down
):
    tok, width = tokens.shape
    top = routes.shape[1]
    cap = max(2, (9 * tok * top + 8 * ep - 1) // (8 * ep))
    cap_pad = -(-cap // 16) * 16
    rows, share, ff, ny = ep * cap_pad, width // tp, w_gate.shape[2], tp // CORES
    sff = s_gate.shape[1]
    sr = sff // ep

    chosen = routes.reshape(tok * top)
    order = jnp.arange(tok * top, dtype=jnp.int32)
    earlier = (chosen[:, None] == chosen[None, :]) & (order[None, :] < order[:, None])
    slot = chosen * cap_pad + jnp.sum(earlier.astype(jnp.int32), axis=1)
    slot_col = slot.reshape(tok, top)

    vm, hbm = pl.BlockSpec(memory_space=pltpu.VMEM), pl.BlockSpec(memory_space=pl.ANY)
    dma, sds = pltpu.SemaphoreType.DMA, jax.ShapeDtypeStruct
    out_shape = [
        sds((tok, share), BF), sds((tok, top), F32), sds((sr, width), F32), sds((2, width), F32),
        sds((ff, 1), F32), sds((sr, 1), F32),
        sds((ep, cap_pad, width), BF), sds((ep, cap_pad, width), BF),
        sds((rows, ff), BF), sds((rows, ff), BF), sds((rows, ff), BF),
    ]
    joint = rows + tok
    scratch = [
        pltpu.VMEM((width, ff), BF), pltpu.VMEM((width, ff), BF), pltpu.VMEM((ff, width), BF),
        pltpu.VMEM((width, sff), BF), pltpu.VMEM((width, sff), BF), pltpu.VMEM((sff, width), BF),
        pltpu.VMEM((2, ep, cap_pad, share), BF),
        pltpu.VMEM((tp, 2, ep, cap_pad, share), BF),
        pltpu.VMEM((3, rows, ff), F32), pltpu.VMEM((rows, ff), F32),
        pltpu.VMEM((ep, sr, width), BF), pltpu.VMEM((ep, sr, width), BF),
        pltpu.VMEM((ny, joint, share), BF), pltpu.VMEM((ny, joint, share), F32),
        pltpu.VMEM((ny, joint, share), BF), pltpu.VMEM((ny, joint, share), BF),
        pltpu.VMEM((ny, joint, share), BF),
        pltpu.VMEM((ep, cap_pad, share), BF), pltpu.VMEM((ep, cap_pad, share), BF),
        pltpu.VMEM((tok, share), F32),
        pltpu.VMEM((ep, 8, 128), F32), pltpu.VMEM((tp, ep, 8, 128), F32),
        pltpu.VMEM((ep, 8, 128), F32), pltpu.VMEM((ep, 8, 128), F32),
        pltpu.VMEM((2, width), F32), pltpu.VMEM((tp, 2, width), F32),
        dma((6,)), dma((2 * tp,)), dma((ep,)), dma((ep,)), dma((ny,)), dma((tp + ny,)), dma((ny,)),
        dma((ep,)), dma((ep,)), dma((ny,)), dma((ny,)), dma((ny,)), dma((ny,)),
        dma((ep,)), dma((ep,)), dma((tp,)), dma((tp,)), dma((ep,)), dma((ep,)), dma((tp,)), dma((tp,)),
    ]
    out = pl.pallas_call(
        functools.partial(body, ep, tp, cap_pad),
        out_shape=out_shape,
        in_specs=[vm] * 5 + [hbm] * 6,
        out_specs=[vm] * 6 + [hbm] * 2 + [vm] * 3,
        scratch_shapes=scratch,
        compiler_params=pltpu.CompilerParams(
            collective_id=0, has_side_effects=True, vmem_limit_bytes=60 * 1024 * 1024
        ),
    )(
        slot_col.T, slot_col, route_gates, tokens, cotangent,
        w_gate[0], w_up[0], w_down[0], s_gate, s_up, s_down,
    )
    token_grad, gate_grad, grad_shared, norm_in, norm_down, norm_sh, x, c, hid, dg, du = out
    x, c = x.reshape(rows, width), c.reshape(rows, width)
    return (
        token_grad, gate_grad, dot(x, dg, 0, 0)[None], dot(x, du, 0, 0)[None],
        dot(hid, c, 0, 0)[None], grad_shared, norm_in[None], norm_down.reshape(1, ff),
        norm_sh.reshape(sr),
    )


def solution(mesh):
    placed = (
        P("ep", None), P("ep", None), P("ep", None), P("ep", None),
        P("ep", None, "tp"), P("ep", None, "tp"), P("ep", "tp", None),
        P(None, "tp"), P(None, "tp"), P("tp", None),
    )
    return jax.shard_map(
        functools.partial(on_device, mesh.shape["ep"], mesh.shape["tp"]),
        mesh=mesh,
        in_specs=placed,
        out_specs=(
            P("ep", "tp"), P("ep", None), P("ep", None, "tp"), P("ep", None, "tp"),
            P("ep", "tp", None), P(("tp", "ep"), None), P("ep", None, None), P("ep", "tp"),
            P(("tp", "ep")),
        ),
        check_vma=False,
    )
```

time: 182 us -> 92.1 us (0.51)
  Pallas kernels: 0 us -> 70.5 us
  blocking collectives: 43 us -> 0 us
  local copies, waits for them, and re-layouts: 44.5 us -> 7.32 us
  waiting for transfers between devices: 27.1 us -> 0 us
  between operations: 15.8 us -> 0.71 us
  matrix products: 24.8 us -> 9.91 us
  starting transfers between devices: 13.9 us -> 0 us
  other arithmetic: 11.5 us -> 3.31 us
    pallas_call x0 -> x1, Pallas kernels: none -> 70.5 us  [on_device(): pl.pallas_call(functools.partial(body, ep, tp, cap_pad), out_shape=out_sh...]
    all_to_all x2 -> x0, blocking collectives: 31.9 us -> none  [the longest x1 18.1 us: on_device(): lax.all_to_all(part_c, 'ep', split_axis=0, concat_axis=0, tiled=True)]
    all_to_all x3 -> x0, waiting for transfers between devices: 18.5 us -> none  [the longest x1 17.8 us: on_device(): lax.all_to_all(slot_part.reshape(ep_count, capacity, model_width), 'ep',...]
    dot_general x12 -> x3, matrix products: 24.8 us -> 9.91 us  [dot(): lax.dot_general(a, b, (((ca,), (cb,)), ((), ())), preferred_element_type=...]
    all_to_all x3 -> x0, starting transfers between devices: 13.8 us -> none  [the longest x1 5.52 us: on_device(): lax.all_to_all(slot_part.reshape(ep_count, capacity, model_width), 'ep',...]
    psum x1 -> x0, blocking collectives: 11.1 us -> none  [on_device(): gate_total, square_total = lax.psum((gate_part, square_part), 'tp')]
    gather x4 -> x0, local copies, waits for them, and re-layouts: 9.18 us -> none  [the longest x1 2.44 us: on_device(): send_x = padded_x[row_token].reshape(ep_count, capacity, model_width)]
    all_gather x2 -> x0, waiting for transfers between devices: 8.63 us -> none  [the longest x1 8.61 us: on_device(): lax.all_gather(moved_x, 'tp', axis=2, tiled=True)]
  transfers between devices with their start and end apart: 6 -> 0, of which waited for: 3 -> 0; matrix products, arithmetic and copies ran while one was open for 36% -> 0% of each run, Pallas kernels for 0% -> 0%
where the time goes in v1:
time: 92.1 us; the launch traced here: 91.8 us
  Pallas kernels  70.5 us (77%)
  matrix products  9.91 us (11%)
  local copies, waits for them, and re-layouts  7.32 us (8%)
  other arithmetic  3.31 us (4%)
    pallas_call x1, Pallas kernels, on_device(): pl.pallas_call(functools.partial(body, ep, tp, cap_pad), out_shape=out_sh...  70.5 us
    dot_general x3, matrix products, dot(): lax.dot_general(a, b, (((ca,), (cb,)), ((), ())), preferred_element_type=...  9.91 us
    unnamed x22, local copies, waits for them, and re-layouts  5.71 us
    pallas_call x2, other arithmetic, on_device(): pl.pallas_call(functools.partial(body, ep, tp, cap_pad), out_shape=out_sh...  2.43 us

profile of v1, /device:TPU:0, one launch (start us, length us, event | category | flops | bytes accessed | tf_op | source)
XLA Modules:
  0.0 91.8 jit_solution(11601309222803978075)
XLA Ops:
  0.6 0.7 broadcast_multiply_fusion
  1.3 0.1 copy.37
  1.4 1.4 %copy.39.gates = f32[128,2]{1,0:T(8,128)} copy(f32[128,2]{0,1:T(2,128)} %param.12) | data formatting | bytes 2048 | tf_op args[2]
  2.9 0.8 copy.36
  3.6 0.1 eq.15
  3.8 0.2 convert_reduce_fusion
  4.0 0.1 reduce_sum.12
  4.1 0.0 copy-start.2
  4.1 0.6 copy.38.slot_row
  4.8 70.5 %shard_map.169 = (bf16[128,512]{1,0:T(8,128)(2,1)}, f32[128,2]{1,0:T(8,128)}, f32[48,2048]{1,0:T(8,128)}, f32[2,2048]{1,0:T(2,128)}, f32[384,1]{1,0:T(8,128)}, /...) custom-call(s32[2,128]{1,0:T(2,128)} %copy.38.slot_row, ...), custom_call_target="tpu_custom_call" | custom-call | tf_op jit(solution)/shard_map/pallas_call | solution.py:348
  75.3 1.4 %reduce.1 = f32[48]{0:T(128)} reduce(f32[48,1]{1,0:T(8,128)} %get-tuple-element.30, f32[]{:T(128)} %constant.7), dimensions={1}, to_apply=%get-tuple-element.30.reduce_sub_computation | reduce | bytes 388 | tf_op jit(solution)/shard_map/pallas_call | solution.py:348
  76.7 1.1 %reduce = f32[384]{0:T(512)S(1)} reduce(f32[384,1]{1,0:T(8,128)} %get-tuple-element.29, f32[]{:T(128)} %constant.7), dimensions={1}, to_apply=%get-tuple-element.29.reduce_sub_computation | reduce | bytes 3076 | tf_op jit(solution)/shard_map/pallas_call | solution.py:348
  77.7 0.6 reshape.37
  78.3 1.5 %copy.40 = f32[128,2]{0,1:T(2,128)} copy(f32[128,2]{1,0:T(8,128)} %get-tuple-element.59) | data formatting | bytes 2048
  79.8 4.4 %convolution_bitcast_fusion.1 = f32[1,2048,384]{2,1,0:T(8,128)} fusion(bf16[384,2048]{1,0:T(8,128)(2,1)} %bitcast.19, bf16[384,384]{1,0:T(8,128)(2,1)} %get-tuple-element.24), kind=kOutput, calls=%fused_computation.1 | convolution fusion | flops 603979776 | bytes 5013504 | tf_op jit(solution)/shard_map/dot_general | solution.py:17
  84.2 0.0 copy-done
  84.2 0.0 copy-start.3
  84.2 2.8 %convolution_bitcast_fusion.2 = f32[1,2048,384]{2,1,0:T(8,128)} fusion(bf16[384,2048]{1,0:T(8,128)(2,1)S(1)} %bitcast.20, bf16[384,384]{1,0:T(8,128)(2,1)S(1)} %copy-done.5), kind=kOutput, calls=%fused_computation.2 | convolution fusion | flops 603979776 | bytes 5013504 | tf_op jit(solution)/shard_map/dot_general | solution.py:17
  87.0 0.0 copy-done.1
  87.1 2.7 %convolution_bitcast_fusion = f32[1,384,2048]{2,1,0:T(8,128)} fusion(bf16[384,384]{1,0:T(8,128)(2,1)S(1)} %copy-done.3, bf16[384,2048]{1,0:T(8,128)(2,1)S(1)} %bitcast.21), kind=kOutput, calls=%fused_computation | convolution fusion | flops 603979776 | bytes 5013504 | tf_op jit(solution)/shard_map/dot_general | solution.py:17
  89.7 0.7 copy.44
  90.4 0.7 copy.45
  91.1 0.0 copy-done.7
  91.1 0.6 copy.46
  (12 shorter events, 0.0 us)
Async XLA Ops:
  4.1 0.7 copy-start.2
  79.8 4.4 %copy-start = (bf16[8,48,2048]{2,1,0:T(8,128)(2,1)S(1)}, bf16[8,48,2048]{2,1,0:T(8,128)(2,1)}, u32[]{:S(2)}) copy-start(bf16[8,48,2048]{2,1,0:T(8,128)(2,1)} %get-tuple-element.22) | copy-start | bytes 4718596
  79.8 4.4 %copy-start.5 = (bf16[384,384]{1,0:T(8,128)(2,1)S(1)}, bf16[384,384]{1,0:T(8,128)(2,1)}, u32[]{:S(2)}) copy-start(bf16[384,384]{1,0:T(8,128)(2,1)} %get-tuple-element.23) | copy-start | bytes 884740
  84.2 2.9 %copy-start.1 = (bf16[8,48,2048]{2,1,0:T(8,128)(2,1)S(1)}, bf16[8,48,2048]{2,1,0:T(8,128)(2,1)}, u32[]{:S(2)}) copy-start(bf16[8,48,2048]{2,1,0:T(8,128)(2,1)} %get-tuple-element.26) | copy-start | bytes 4718596
  84.2 2.8 %copy-start.3 = (bf16[384,384]{1,0:T(8,128)(2,1)S(1)}, bf16[384,384]{1,0:T(8,128)(2,1)}, u32[]{:S(2)}) copy-start(bf16[384,384]{1,0:T(8,128)(2,1)} %get-tuple-element.25) | copy-start | bytes 884740
  87.0 2.7 %copy-start.6 = (bf16[128,512]{1,0:T(8,128)(2,1)S(1)}, bf16[128,512]{1,0:T(8,128)(2,1)}, u32[]{:S(2)}) copy-start(bf16[128,512]{1,0:T(8,128)(2,1)} %get-tuple-element.76) | copy-start | bytes 393220
  87.0 3.3 %copy-start.4 = (f32[48,2048]{1,0:T(8,128)S(1)}, f32[48,2048]{1,0:T(8,128)}, u32[]{:S(2)}) copy-start(f32[48,2048]{1,0:T(8,128)} %get-tuple-element.81) | copy-start | bytes 1179652
  87.1 4.1 %copy-start.7 = (f32[2,2048]{1,0:T(2,128)S(1)}, f32[2,2048]{1,0:T(2,128)}, u32[]{:S(2)}) copy-start(f32[2,2048]{1,0:T(2,128)} %get-tuple-element.28) | copy-start | bytes 49156

commit v2 on v1

v2 whole, which is shorter than its diff:
```python
import functools

import jax
import jax.numpy as jnp
from jax import lax
from jax.experimental import pallas as pl
from jax.experimental.pallas import tpu as pltpu
from jax.sharding import PartitionSpec as P

MESH = pl.DeviceIdType.MESH
CORES = 2
BF = jnp.bfloat16
F32 = jnp.float32


def dot(a, b, ca=1, cb=0):
    return lax.dot_general(a, b, (((ca,), (cb,)), ((), ())), preferred_element_type=F32)


def activations(pre_gate, pre_up, hidden_grad):
    sig = jax.nn.sigmoid(pre_gate)
    act = pre_gate * sig
    hidden = (act * pre_up).astype(BF)
    d_gate = (hidden_grad * pre_up * sig * (1.0 + pre_gate * (1.0 - sig))).astype(BF)
    d_up = (hidden_grad * act).astype(BF)
    return hidden, d_gate, d_up


def body(
    ep, tp, cap_pad, live,
    routes, gate_rows, tokens, cot, wg_h, wu_h, wd_h, sg_h, su_h, sd_h,
    token_out, gate_out, shared_out, norm_in_out, norm_down_out, norm_sh_out,
    x_out, c_out, hid_out, dg_out, du_out,
    wg, wu, wd, sg, su, sd, send, rx, acc, prod, term, term_rx, pair, pair_rx,
    part_a, part_own, recv_a, part_b, recv_b, sh_a, sh_own, sh_recv_a, sh_b, sh_recv_b,
    back_tx, back_rx, gpart, grecv, gsend, gback, sq, sq_rx,
    w_sem, out_sem, d1_s, d1_r, d2_s, d2_r, pass_s, rs_s, rs_r, rp_s, rp_r, ra_s, ra_r, rb_s, rb_r,
    bk_s, bk_r, g_s, g_r, gb_s, gb_r, q_s, q_r, sa_s, sa_r, sb_s, sb_r,
):
    me = lax.axis_index("ep")
    j = lax.axis_index("tp")
    core = lax.rem(j, CORES)
    y = lax.div(j, CORES)
    mate = j + 1 - 2 * core
    ny = tp // CORES
    rows = ep * cap_pad
    tok, width = tokens.shape
    share = width // tp
    top = routes.shape[0]
    px = lax.rem(me, 2)
    group = lax.div(me, 2)
    groups = ep // 2
    ff = wg.shape[1]
    sr = shared_out.shape[0]

    loads = [
        pltpu.make_async_copy(src, dst, w_sem.at[n])
        for n, (src, dst) in enumerate(
            [(sg_h, sg), (su_h, su), (sd_h, sd), (wg_h, wg), (wu_h, wu), (wd_h, wd)]
        )
    ]
    for load in loads:
        load.start()

    def ep_peer(step):
        return lax.rem(me + step, ep)

    def remote(src, dst, ssem, rsem, **where):
        copy = pltpu.make_async_remote_copy(
            src_ref=src, dst_ref=dst, send_sem=ssem, recv_sem=rsem,
            device_id=where, device_id_type=MESH,
        )
        copy.start()
        return copy

    barrier = pltpu.get_barrier_semaphore()
    for step in range(1, ep):
        pl.semaphore_signal(barrier, inc=1, device_id={"ep": ep_peer(step)}, device_id_type=MESH)
    for step in range(1, tp):
        pl.semaphore_signal(
            barrier, inc=1, device_id={"tp": lax.rem(j + step, tp)}, device_id_type=MESH
        )

    if live < cap_pad:
        rx[:, :, :, live:, :] = jnp.zeros((tp, 2, ep, cap_pad - live, share), BF)
        back_rx[:, live:, :] = jnp.zeros((ep, cap_pad - live, share), BF)

    sub = lax.broadcasted_iota(jnp.int32, (tok, tok), 0)
    lane = lax.broadcasted_iota(jnp.int32, (tok, tok), 1)

    def to_col(row):
        return jnp.sum(jnp.where(sub == lane, row, 0.0), axis=1, keepdims=True)

    def to_row(col):
        return jnp.sum(jnp.where(sub == lane, col, 0.0), axis=0, keepdims=True)

    expert_row = [routes[k : k + 1, :].astype(F32) for k in range(top)]
    expert_col = [to_col(row) for row in expert_row]
    gate_col = [to_col(gate_rows[k : k + 1, :]) for k in range(top)]
    slot_row = []
    for k in range(top):
        slot = expert_row[k] * cap_pad
        for other in range(top):
            same = (expert_col[other] == expert_row[k]) & (sub < lane)
            slot = slot + jnp.sum(jnp.where(same, 1.0, 0.0), axis=0, keepdims=True)
        slot_row.append(slot)
    slot_col = [to_col(row) for row in slot_row]

    cols = pl.ds(pl.multiple_of(j * share, share), share)
    x_share = tokens[:, cols]
    c_share = cot[:, cols].astype(F32)
    slot_ids = lax.broadcasted_iota(jnp.int32, (rows, tok), 0).astype(F32)
    any_hot = jnp.zeros((rows, tok), F32)
    c_rows = jnp.zeros((rows, share), F32)
    for k in range(top):
        hot = jnp.where(slot_ids == slot_row[k], 1.0, 0.0)
        any_hot = any_hot + hot
        c_rows = c_rows + dot(hot.astype(BF), (gate_col[k] * c_share).astype(BF))
    x_rows = dot(any_hot.astype(BF), x_share)
    send[0] = x_rows.astype(BF).reshape(ep, cap_pad, share)
    send[1] = c_rows.astype(BF).reshape(ep, cap_pad, share)

    pl.semaphore_wait(barrier, ep + tp - 2)

    filled = pl.ds(0, live)
    far_first = sorted(range(1, ep), key=lambda step: -min(step, ep - step))
    waits, d1 = [], {}
    for step in far_first:
        to = ep_peer(step)
        d1[step] = remote(
            send.at[:, to, filled], rx.at[j, :, me, filled], d1_s.at[step], d1_r.at[step], ep=to
        )
        waits.append(d1[step])
    rx[j, :, me] = send[:, me]

    def forward(source):
        block = rx.at[j, :, source, filled]
        remote(block, block, d2_s.at[0], d2_r.at[j], tp=mate)
        for step in range(1, ny):
            to = lax.rem(y + step, ny) * CORES + core
            remote(block, block, d2_s.at[step], d2_r.at[j], tp=to)

    forward(me)

    def part_of(block, d_gate, d_up, gate_w, up_w):
        at = pl.ds(pl.multiple_of(block * share, share), share)
        return dot(d_gate, gate_w[at, :], 1, 1) + dot(d_up, up_w[at, :], 1, 1)

    far_y = [lax.rem(y + step, ny) for step in range(1, ny)] + [y]

    held, sa, rs = {}, [], []

    def shared_gate():
        loads[0].wait()
        held["gate"] = dot(tokens[...], sg[...])

    def shared_up():
        loads[1].wait()
        held["up"] = dot(tokens[...], su[...])

    def shared_act():
        loads[2].wait()
        held["act"] = activations(held["gate"], held["up"], dot(cot[...], sd[...], 1, 1))

    def shared_term(chunks):
        for chunk in chunks:
            at = slice(chunk * share, (chunk + 1) * share)
            value = dot(held["act"][0], cot[:, at], 0, 0)
            for i in range(ep):
                term[i % 2, i // 2, :, at] = value[i * sr : (i + 1) * sr].astype(BF)

    def shared_send():
        for d in range(groups):
            rs.append(
                remote(
                    term.at[1 - px, d], term_rx.at[d], rs_s.at[d], rs_r.at[d],
                    ep=me + 1 - 2 * px,
                )
            )

    def shared_parts():
        for n, yq in enumerate(far_y):
            sh_a[n] = part_of(yq * CORES + 1 - core, *held["act"][1:], sg, su).astype(BF)
            sa.append(remote(sh_a.at[n], sh_recv_a.at[n], sa_s.at[n], sa_r.at[n], tp=mate))

    def shared_own():
        for n, yq in enumerate(far_y):
            sh_own[n] = part_of(yq * CORES + core, *held["act"][1:], sg, su)

    tasks = [
        shared_gate, shared_up, shared_act, lambda: shared_term(range(tp // 2)),
        lambda: (shared_term(range(tp // 2, tp)), shared_send()), shared_parts, shared_own,
    ]
    stride = -(-(ep - 1) // len(tasks))
    for n, task in enumerate(tasks):
        task()
        for step in far_first[n * stride : (n + 1) * stride]:
            d1[step].wait_recv()
            forward(lax.rem(me - step + ep, ep))

    for load in loads[3:]:
        load.wait()
    acc[...] = jnp.zeros_like(acc)

    def add_share(t):
        at = pl.ds(pl.multiple_of(t * share, share), share)
        x_in = rx[t, 0].reshape(rows, share)
        c_in = rx[t, 1].reshape(rows, share)
        acc[0] += dot(x_in, wg[at, :])
        acc[1] += dot(x_in, wu[at, :])
        acc[2] += dot(c_in, wd[:, at], 1, 1)

    def arrived(t):
        pltpu.make_async_remote_copy(
            src_ref=rx.at[t, :, :, filled], dst_ref=rx.at[t, :, :, filled],
            send_sem=d2_s.at[0], recv_sem=d2_r.at[t],
            device_id={"tp": mate}, device_id_type=MESH,
        ).wait_recv()

    add_share(j)
    passed = []
    for step in range(1, ny):
        t = lax.rem(y - step + ny, ny) * CORES + core
        arrived(t)
        whole = rx.at[t, :, :, filled]
        passed.append(remote(whole, whole, pass_s.at[step], d2_r.at[tp + step], tp=mate))
        if step == 1:
            arrived(mate)
            add_share(mate)
        add_share(t)
    for step in range(1, ny):
        t = lax.rem(y - step + ny, ny) * CORES + 1 - core
        passed[step - 1].wait_recv()
        add_share(t)

    sb = []
    for n, yq in enumerate(far_y[:-1]):
        sa[n].wait_recv()
        sh_b[n] = (sh_own[n] + sh_recv_a[n].astype(F32)).astype(BF)
        sb.append(
            remote(sh_b.at[n], sh_recv_b.at[n], sb_s.at[n], sb_r.at[n], tp=yq * CORES + core)
        )

    outs = []
    for t in range(tp):
        at = pl.ds(t * share, share)
        outs.append(pltpu.make_async_copy(rx.at[t, 0], x_out.at[:, :, at], out_sem.at[2 * t]))
        outs.append(pltpu.make_async_copy(rx.at[t, 1], c_out.at[:, :, at], out_sem.at[2 * t + 1]))
    for out in outs:
        out.start()

    hidden, d_gate, d_up = activations(acc[0], acc[1], acc[2])
    hid_out[...] = hidden
    dg_out[...] = d_gate
    du_out[...] = d_up
    prod[...] = hidden.astype(F32) * acc[2]

    ra = []
    for n, yq in enumerate(far_y):
        value = part_of(yq * CORES + 1 - core, d_gate, d_up, wg, wu).astype(BF)
        part_a[n] = value.reshape(ep, cap_pad, share)
        ra.append(
            remote(part_a.at[n, :, filled], recv_a.at[n, :, filled], ra_s.at[n], ra_r.at[n], tp=mate)
        )
    rb = []
    for n, yq in enumerate(far_y):
        value = part_of(yq * CORES + core, d_gate, d_up, wg, wu)
        part_own[n] = value.reshape(ep, cap_pad, share)
        if n < ny - 1:
            ra[n].wait_recv()
            part_b[n] = (part_own[n] + recv_a[n].astype(F32)).astype(BF)
            rb.append(
                remote(
                    part_b.at[n, :, filled], recv_b.at[n, :, filled], rb_s.at[n], rb_r.at[n],
                    tp=yq * CORES + core,
                )
            )

    rp = []
    for d in range(groups):
        rs[d].wait_recv()
    for step in range(groups):
        d = lax.rem(group + step, groups)
        pair[d] = (term[px, d].astype(F32) + term_rx[d].astype(F32)).astype(BF)
        if step > 0:
            rp.append(
                remote(
                    pair.at[d], pair_rx.at[group], rp_s.at[step], rp_r.at[step], ep=2 * d + px
                )
            )
    pair_rx[group] = pair[group]

    gpart[...] = jnp.zeros_like(gpart)
    ones = jnp.ones((8, ff), F32)
    for i in range(ep):
        gpart[i, :, :cap_pad] = lax.dot_general(
            ones, prod[i * cap_pad : (i + 1) * cap_pad, :], (((1,), (1,)), ((), ())),
            preferred_element_type=F32, precision=lax.Precision.HIGHEST,
        )
    gx = []
    for step in range(1, tp):
        gx.append(remote(gpart, grecv.at[step], g_s.at[step], g_r.at[step], tp=lax.rem(j + step, tp)))

    for copy in gx:
        copy.wait_recv()
    total = gpart[...]
    for step in range(1, tp):
        total = total + grecv[step]
    gsend[...] = total.astype(BF).astype(F32)
    gb = []
    for step in range(1, ep):
        to = ep_peer(step)
        gb.append(remote(gsend.at[to], gback.at[me], gb_s.at[step], gb_r.at[step], ep=to))
    gback[me] = gsend[me]

    ra[ny - 1].wait_recv()
    part = part_own[ny - 1] + recv_a[ny - 1].astype(F32)
    for n in range(ny - 1):
        rb[n].wait_recv()
        part = part + recv_b[n].astype(F32)
    back_tx[...] = part.astype(BF)
    bk = []
    for step in range(1, ep):
        to = ep_peer(step)
        bk.append(
            remote(
                back_tx.at[to, filled], back_rx.at[me, filled], bk_s.at[step], bk_r.at[step], ep=to
            )
        )
    back_rx[me, :live] = back_tx[me, :live]

    sa[ny - 1].wait_recv()
    shared_tot = sh_own[ny - 1] + sh_recv_a[ny - 1].astype(F32)
    for n in range(ny - 1):
        sb[n].wait_recv()
        shared_tot = shared_tot + sh_recv_b[n].astype(F32)

    norm_down = jnp.zeros((1, ff), F32)
    for t in range(tp):
        at = slice(t * share, (t + 1) * share)
        x_in = rx[t, 0].reshape(rows, share)
        c_in = rx[t, 1].reshape(rows, share)
        sq[0:1, at] = jnp.sum(jnp.square(dot(dg_out[...], x_in, 0, 0)), axis=0, keepdims=True)
        sq[1:2, at] = jnp.sum(jnp.square(dot(du_out[...], x_in, 0, 0)), axis=0, keepdims=True)
        norm_down += jnp.sum(jnp.square(dot(c_in, hid_out[...], 0, 0)), axis=0, keepdims=True)
    norm_down_out[...] = norm_down / width
    qx = []
    for step in range(1, tp):
        qx.append(remote(sq, sq_rx.at[step], q_s.at[step], q_r.at[step], tp=lax.rem(j + step, tp)))

    for copy in qx:
        copy.wait_recv()
    squares = sq[...]
    for step in range(1, tp):
        squares = squares + sq_rx[step]
    norm_in_out[...] = squares / (tp * ff)

    for copy in rp:
        copy.wait_recv()
    grad = pair_rx[0].astype(F32)
    for i in range(1, groups):
        grad = grad + pair_rx[i].astype(F32)
    shared_out[...] = grad
    norm_sh = jnp.mean(jnp.square(grad), axis=1, keepdims=True)
    here = lax.broadcasted_iota(jnp.int32, (sr, sr), 0) == lax.broadcasted_iota(
        jnp.int32, (sr, sr), 1
    )
    norm_sh_out[...] = jnp.sum(jnp.where(here, norm_sh, 0.0), axis=0, keepdims=True)

    for copy in gb:
        copy.wait_recv()
    spot = lax.broadcasted_iota(jnp.int32, (tok, 128), 1)
    spot_f = spot.astype(F32)
    for k in range(top):
        picked = jnp.zeros((tok, 128), F32)
        for i in range(ep):
            hit = (spot < cap_pad) & (slot_col[k] == spot_f + float(i * cap_pad))
            picked = picked + jnp.where(hit, gback[i, 0:1, :], 0.0)
        dots = to_row(jnp.sum(picked, axis=1, keepdims=True))
        gate_out[k : k + 1, :] = dots / gate_rows[k : k + 1, :]

    place = lax.broadcasted_iota(jnp.int32, (tok, rows), 1).astype(F32)
    pick = jnp.zeros((tok, rows), F32)
    for k in range(top):
        pick = pick + jnp.where(place == slot_col[k], 1.0, 0.0)
    for copy in bk:
        copy.wait_recv()
    token_out[...] = (
        dot(pick.astype(BF), back_rx[...].reshape(rows, share)) + shared_tot
    ).astype(BF)

    sent = rx.at[j, :, :, filled]
    for step in range(ny):
        pltpu.make_async_remote_copy(
            src_ref=sent, dst_ref=sent, send_sem=d2_s.at[step], recv_sem=d2_r.at[j],
            device_id={"tp": mate}, device_id_type=MESH,
        ).wait_send()
    for copy in waits + passed + ra + gx + rb + qx + gb + bk + rs + rp + sa + sb:
        copy.wait_send()
    for out in outs:
        out.wait()


def on_device(
    ep, tp, tokens, routes, route_gates, cotangent, w_gate, w_up, w_down, s_gate, s_up, s_down
):
    tok, width = tokens.shape
    top = routes.shape[1]
    cap = max(2, (9 * tok * top + 8 * ep - 1) // (8 * ep))
    cap_pad = -(-cap // 16) * 16
    rows, share, ff, ny = ep * cap_pad, width // tp, w_gate.shape[2], tp // CORES
    sff = s_gate.shape[1]
    sr = sff // ep

    live = -(-cap // 8) * 8

    vm, hbm = pl.BlockSpec(memory_space=pltpu.VMEM), pl.BlockSpec(memory_space=pl.ANY)
    dma, sds = pltpu.SemaphoreType.DMA, jax.ShapeDtypeStruct
    out_shape = [
        sds((tok, share), BF), sds((top, tok), F32), sds((sr, width), F32), sds((2, width), F32),
        sds((1, ff), F32), sds((1, sr), F32),
        sds((ep, cap_pad, width), BF), sds((ep, cap_pad, width), BF),
        sds((rows, ff), BF), sds((rows, ff), BF), sds((rows, ff), BF),
    ]
    slots = (ny, ep, cap_pad, share)
    scratch = [
        pltpu.VMEM((width, ff), BF), pltpu.VMEM((width, ff), BF), pltpu.VMEM((ff, width), BF),
        pltpu.VMEM((width, sff), BF), pltpu.VMEM((width, sff), BF), pltpu.VMEM((sff, width), BF),
        pltpu.VMEM((2, ep, cap_pad, share), BF),
        pltpu.VMEM((tp, 2, ep, cap_pad, share), BF),
        pltpu.VMEM((3, rows, ff), F32), pltpu.VMEM((rows, ff), F32),
        pltpu.VMEM((2, ep // 2, sr, width), BF), pltpu.VMEM((ep // 2, sr, width), BF),
        pltpu.VMEM((ep // 2, sr, width), BF), pltpu.VMEM((ep // 2, sr, width), BF),
        pltpu.VMEM(slots, BF), pltpu.VMEM(slots, F32), pltpu.VMEM(slots, BF),
        pltpu.VMEM(slots, BF), pltpu.VMEM(slots, BF),
        pltpu.VMEM((ny, tok, share), BF), pltpu.VMEM((ny, tok, share), F32),
        pltpu.VMEM((ny, tok, share), BF), pltpu.VMEM((ny, tok, share), BF),
        pltpu.VMEM((ny, tok, share), BF),
        pltpu.VMEM((ep, cap_pad, share), BF), pltpu.VMEM((ep, cap_pad, share), BF),
        pltpu.VMEM((ep, 8, 128), F32), pltpu.VMEM((tp, ep, 8, 128), F32),
        pltpu.VMEM((ep, 8, 128), F32), pltpu.VMEM((ep, 8, 128), F32),
        pltpu.VMEM((2, width), F32), pltpu.VMEM((tp, 2, width), F32),
        dma((6,)), dma((2 * tp,)), dma((ep,)), dma((ep,)), dma((ny,)), dma((tp + ny,)), dma((ny,)),
        dma((ep,)), dma((ep,)), dma((ep,)), dma((ep,)), dma((ny,)), dma((ny,)), dma((ny,)), dma((ny,)),
        dma((ep,)), dma((ep,)), dma((tp,)), dma((tp,)), dma((ep,)), dma((ep,)), dma((tp,)), dma((tp,)),
        dma((ny,)), dma((ny,)), dma((ny,)), dma((ny,)),
    ]
    out = pl.pallas_call(
        functools.partial(body, ep, tp, cap_pad, live),
        out_shape=out_shape,
        in_specs=[vm] * 4 + [hbm] * 6,
        out_specs=[vm] * 6 + [hbm] * 2 + [vm] * 3,
        scratch_shapes=scratch,
        compiler_params=pltpu.CompilerParams(
            collective_id=0, has_side_effects=True, vmem_limit_bytes=60 * 1024 * 1024
        ),
    )(
        routes.T, route_gates.T, tokens, cotangent,
        w_gate[0], w_up[0], w_down[0], s_gate, s_up, s_down,
    )
    token_grad, gate_grad, grad_shared, norm_in, norm_down, norm_sh, x, c, hid, dg, du = out
    x, c = x.reshape(rows, width), c.reshape(rows, width)
    return (
        token_grad, gate_grad.T, dot(x, dg, 0, 0)[None], dot(x, du, 0, 0)[None],
        dot(hid, c, 0, 0)[None], grad_shared, norm_in[None], norm_down.reshape(1, ff),
        norm_sh.reshape(sr),
    )


def solution(mesh):
    placed = (
        P("ep", None), P("ep", None), P("ep", None), P("ep", None),
        P("ep", None, "tp"), P("ep", None, "tp"), P("ep", "tp", None),
        P(None, "tp"), P(None, "tp"), P("tp", None),
    )
    return jax.shard_map(
        functools.partial(on_device, mesh.shape["ep"], mesh.shape["tp"]),
        mesh=mesh,
        in_specs=placed,
        out_specs=(
            P("ep", "tp"), P("ep", None), P("ep", None, "tp"), P("ep", None, "tp"),
            P("ep", "tp", None), P(("tp", "ep"), None), P("ep", None, None), P("ep", "tp"),
            P(("tp", "ep")),
        ),
        check_vma=False,
    )
```

time: 92.1 us -> 79.4 us (0.86)
  Pallas kernels: 70.5 us -> 64.5 us
  local copies, waits for them, and re-layouts: 7.32 us -> 3.68 us
  other arithmetic: 3.31 us -> 0 us
    pallas_call x1, Pallas kernels: 70.5 us -> 64.5 us  [on_device(): pl.pallas_call(functools.partial(body, ep, tp, cap_pad, live), out_shape=...]
    pallas_call x2 -> x0, other arithmetic: 2.43 us -> none  [on_device(): pl.pallas_call(functools.partial(body, ep, tp, cap_pad), out_shape=out_sh...]
    unnamed x22 -> x26, local copies, waits for them, and re-layouts: 5.71 us -> 3.68 us
where the time goes in v2:
time: 79.4 us; the launch traced here: 79 us
  Pallas kernels  64.5 us (81%)
  matrix products  10.1 us (13%)
  local copies, waits for them, and re-layouts  3.68 us (5%)
    pallas_call x1, Pallas kernels, on_device(): pl.pallas_call(functools.partial(body, ep, tp, cap_pad, live), out_shape=...  64.5 us
    dot_general x3, matrix products, dot(): lax.dot_general(a, b, (((ca,), (cb,)), ((), ())), preferred_element_type=...  10.1 us
    unnamed x26, local copies, waits for them, and re-layouts  3.68 us

profile of v2, /device:TPU:0, one launch (start us, length us, event | category | flops | bytes accessed | tf_op | source)
XLA Modules:
  0.0 79.0 jit_solution(5746672130920473398)
XLA Ops:
  0.6 64.5 %shard_map.169 = (bf16[128,512]{1,0:T(8,128)(2,1)}, f32[2,128]{1,0:T(2,128)}, f32[48,2048]{1,0:T(8,128)}, f32[2,2048]{1,0:T(2,128)}, f32[1,384]{1,0:T(1,128)}, /...) custom-call(s32[2,128]{1,0:T(2,128)} %bitcast.29, ...), custom_call_target="tpu_custom_call" | custom-call | tf_op jit(solution)/shard_map/pallas_call | solution.py:448
  65.1 0.0 copy-start
  65.2 0.0 copy-start.4
  65.2 4.6 %convolution_bitcast_fusion.1 = f32[1,2048,384]{2,1,0:T(8,128)} fusion(bf16[384,2048]{1,0:T(8,128)(2,1)} %bitcast.22, bf16[384,384]{1,0:T(8,128)(2,1)} %get-tuple-element.24), kind=kOutput, calls=%fused_computation.1 | convolution fusion | flops 603979776 | bytes 5013504 | tf_op jit(solution)/shard_map/dot_general | solution.py:17
  69.8 0.0 copy-done
  69.8 0.0 copy-done.4
  69.8 0.0 copy-start.2
  69.8 2.8 %convolution_bitcast_fusion.2 = f32[1,2048,384]{2,1,0:T(8,128)} fusion(bf16[384,2048]{1,0:T(8,128)(2,1)S(1)} %bitcast.23, bf16[384,384]{1,0:T(8,128)(2,1)S(1)} %copy-done.4), kind=kOutput, calls=%fused_computation.2 | convolution fusion | flops 603979776 | bytes 5013504 | tf_op jit(solution)/shard_map/dot_general | solution.py:17
  72.6 0.0 copy-done.1
  72.6 0.0 copy-done.2
  72.6 0.0 copy-start.3
  72.7 0.0 copy-start.6
  72.7 0.0 copy-start.7
  72.7 0.0 copy-start.9
  72.7 2.7 %convolution_bitcast_fusion = f32[1,384,2048]{2,1,0:T(8,128)} fusion(bf16[384,384]{1,0:T(8,128)(2,1)S(1)} %copy-done.2, bf16[384,2048]{1,0:T(8,128)(2,1)S(1)} %bitcast.24), kind=kOutput, calls=%fused_computation | convolution fusion | flops 603979776 | bytes 5013504 | tf_op jit(solution)/shard_map/dot_general | solution.py:17
  75.4 0.7 copy.25
  76.0 0.6 copy.26
  76.6 0.7 copy.27
  77.3 0.0 copy-done.6
  77.3 0.6 copy.28
  77.9 0.0 copy-done.7
  77.9 0.6 copy.29
  78.5 0.0 copy-done.9
  78.5 0.5 copy.30
  (6 shorter events, 0.0 us)
Async XLA Ops:
  65.1 4.6 %copy-start = (bf16[8,48,2048]{2,1,0:T(8,128)(2,1)S(1)}, bf16[8,48,2048]{2,1,0:T(8,128)(2,1)}, u32[]{:S(2)}) copy-start(bf16[8,48,2048]{2,1,0:T(8,128)(2,1)} %get-tuple-element.22) | copy-start | bytes 4718596
  65.2 4.6 %copy-start.4 = (bf16[384,384]{1,0:T(8,128)(2,1)S(1)}, bf16[384,384]{1,0:T(8,128)(2,1)}, u32[]{:S(2)}) copy-start(bf16[384,384]{1,0:T(8,128)(2,1)} %get-tuple-element.23) | copy-start | bytes 884740
  69.8 2.9 %copy-start.1 = (bf16[8,48,2048]{2,1,0:T(8,128)(2,1)S(1)}, bf16[8,48,2048]{2,1,0:T(8,128)(2,1)}, u32[]{:S(2)}) copy-start(bf16[8,48,2048]{2,1,0:T(8,128)(2,1)} %get-tuple-element.26) | copy-start | bytes 4718596
  69.8 2.9 %copy-start.2 = (bf16[384,384]{1,0:T(8,128)(2,1)S(1)}, bf16[384,384]{1,0:T(8,128)(2,1)}, u32[]{:S(2)}) copy-start(bf16[384,384]{1,0:T(8,128)(2,1)} %get-tuple-element.25) | copy-start | bytes 884740
  72.6 2.7 %copy-start.5 = (bf16[128,512]{1,0:T(8,128)(2,1)S(1)}, bf16[128,512]{1,0:T(8,128)(2,1)}, u32[]{:S(2)}) copy-start(bf16[128,512]{1,0:T(8,128)(2,1)} %get-tuple-element.40) | copy-start | bytes 393220
  72.6 3.4 %copy-start.8 = (f32[2,128]{1,0:T(2,128)S(1)}, f32[2,128]{1,0:T(2,128)}, u32[]{:S(2)}) copy-start(f32[2,128]{1,0:T(2,128)} %get-tuple-element.21) | copy-start | bytes 3076
  72.6 3.9 %copy-start.3 = (f32[48,2048]{1,0:T(8,128)S(1)}, f32[48,2048]{1,0:T(8,128)}, u32[]{:S(2)}) copy-start(f32[48,2048]{1,0:T(8,128)} %get-tuple-element.45) | copy-start | bytes 1179652
  72.7 4.7 %copy-start.6 = (f32[2,2048]{1,0:T(2,128)S(1)}, f32[2,2048]{1,0:T(2,128)}, u32[]{:S(2)}) copy-start(f32[2,2048]{1,0:T(2,128)} %get-tuple-element.28) | copy-start | bytes 49156
  72.7 5.3 %copy-start.7 = (f32[1,384]{1,0:T(1,128)S(1)}, f32[1,384]{1,0:T(1,128)}, u32[]{:S(2)}) copy-start(f32[1,384]{1,0:T(1,128)} %get-tuple-element.47) | copy-start | bytes 4612
  72.7 5.8 %copy-start.9 = (f32[1,48]{1,0:T(1,128)S(1)}, f32[1,48]{1,0:T(1,128)}, u32[]{:S(2)}) copy-start(f32[1,48]{1,0:T(1,128)} %get-tuple-element.30) | copy-start | bytes 580

commit v3 on v2

--- a/solution.py
+++ b/solution.py
@@ -233,6 +233,20 @@
         passed[step - 1].wait_recv()
         add_share(t)
 
+    rp = []
+    for d in range(groups):
+        rs[d].wait_recv()
+    for step in range(groups):
+        d = lax.rem(group + step, groups)
+        pair[d] = (term[px, d].astype(F32) + term_rx[d].astype(F32)).astype(BF)
+        if step > 0:
+            rp.append(
+                remote(
+                    pair.at[d], pair_rx.at[group], rp_s.at[step], rp_r.at[step], ep=2 * d + px
+                )
+            )
+    pair_rx[group] = pair[group]
+
     sb = []
     for n, yq in enumerate(far_y[:-1]):
         sa[n].wait_recv()
@@ -275,20 +289,6 @@
                     tp=yq * CORES + core,
                 )
             )
-
-    rp = []
-    for d in range(groups):
-        rs[d].wait_recv()
-    for step in range(groups):
-        d = lax.rem(group + step, groups)
-        pair[d] = (term[px, d].astype(F32) + term_rx[d].astype(F32)).astype(BF)
-        if step > 0:
-            rp.append(
-                remote(
-                    pair.at[d], pair_rx.at[group], rp_s.at[step], rp_r.at[step], ep=2 * d + px
-                )
-            )
-    pair_rx[group] = pair[group]
 
     gpart[...] = jnp.zeros_like(gpart)
     ones = jnp.ones((8, ff), F32)

time: 79.4 us -> 78.6 us (0.990)
  Pallas kernels: 64.5 us -> 63.6 us
    pallas_call x1, Pallas kernels: 64.5 us -> 63.6 us  [on_device(): pl.pallas_call(functools.partial(body, ep, tp, cap_pad, live), out_shape=...]
where the time goes in v3:
time: 78.6 us; the launch traced here: 77.9 us
  Pallas kernels  63.6 us (81%)
  matrix products  9.92 us (13%)
  local copies, waits for them, and re-layouts  3.68 us (5%)
    pallas_call x1, Pallas kernels, on_device(): pl.pallas_call(functools.partial(body, ep, tp, cap_pad, live), out_shape=...  63.6 us
    dot_general x3, matrix products, dot(): lax.dot_general(a, b, (((ca,), (cb,)), ((), ())), preferred_element_type=...  9.92 us
    unnamed x26, local copies, waits for them, and re-layouts  3.68 us

profile of v3, /device:TPU:0, one launch (start us, length us, event | category | flops | bytes accessed | tf_op | source)
XLA Modules:
  0.0 77.9 jit_solution(9133091976909105431)
XLA Ops:
  0.6 63.6 %shard_map.169 = (bf16[128,512]{1,0:T(8,128)(2,1)}, f32[2,128]{1,0:T(2,128)}, f32[48,2048]{1,0:T(8,128)}, f32[2,2048]{1,0:T(2,128)}, f32[1,384]{1,0:T(1,128)}, /...) custom-call(s32[2,128]{1,0:T(2,128)} %bitcast.29, ...), custom_call_target="tpu_custom_call" | custom-call | tf_op jit(solution)/shard_map/pallas_call | solution.py:448
  64.2 0.0 copy-start
  64.2 0.0 copy-start.4
  64.2 4.4 %convolution_bitcast_fusion.1 = f32[1,2048,384]{2,1,0:T(8,128)} fusion(bf16[384,2048]{1,0:T(8,128)(2,1)} %bitcast.22, bf16[384,384]{1,0:T(8,128)(2,1)} %get-tuple-element.24), kind=kOutput, calls=%fused_computation.1 | convolution fusion | flops 603979776 | bytes 5013504 | tf_op jit(solution)/shard_map/dot_general | solution.py:17
  68.6 0.0 copy-done
  68.6 0.0 copy-done.4
  68.7 0.0 copy-start.2
  68.7 2.8 %convolution_bitcast_fusion.2 = f32[1,2048,384]{2,1,0:T(8,128)} fusion(bf16[384,2048]{1,0:T(8,128)(2,1)S(1)} %bitcast.23, bf16[384,384]{1,0:T(8,128)(2,1)S(1)} %copy-done.4), kind=kOutput, calls=%fused_computation.2 | convolution fusion | flops 603979776 | bytes 5013504 | tf_op jit(solution)/shard_map/dot_general | solution.py:17
  71.5 0.0 copy-done.1
  71.5 0.0 copy-done.2
  71.5 0.0 copy-start.3
  71.5 0.0 copy-start.6
  71.5 0.0 copy-start.7
  71.5 0.0 copy-start.9
  71.6 2.7 %convolution_bitcast_fusion = f32[1,384,2048]{2,1,0:T(8,128)} fusion(bf16[384,384]{1,0:T(8,128)(2,1)S(1)} %copy-done.2, bf16[384,2048]{1,0:T(8,128)(2,1)S(1)} %bitcast.24), kind=kOutput, calls=%fused_computation | convolution fusion | flops 603979776 | bytes 5013504 | tf_op jit(solution)/shard_map/dot_general | solution.py:17
  74.2 0.0 copy-done.5
  74.2 0.7 copy.25
  74.9 0.0 copy-done.8
  74.9 0.6 copy.26
  75.5 0.0 copy-done.3
  75.5 0.7 copy.27
  76.2 0.6 copy.28
  76.8 0.6 copy.29
  77.4 0.5 copy.30
  (6 shorter events, 0.0 us)
Async XLA Ops:
  64.2 4.4 %copy-start = (bf16[8,48,2048]{2,1,0:T(8,128)(2,1)S(1)}, bf16[8,48,2048]{2,1,0:T(8,128)(2,1)}, u32[]{:S(2)}) copy-start(bf16[8,48,2048]{2,1,0:T(8,128)(2,1)} %get-tuple-element.22) | copy-start | bytes 4718596
  64.2 4.4 %copy-start.4 = (bf16[384,384]{1,0:T(8,128)(2,1)S(1)}, bf16[384,384]{1,0:T(8,128)(2,1)}, u32[]{:S(2)}) copy-start(bf16[384,384]{1,0:T(8,128)(2,1)} %get-tuple-element.23) | copy-start | bytes 884740
  68.7 2.9 %copy-start.1 = (bf16[8,48,2048]{2,1,0:T(8,128)(2,1)S(1)}, bf16[8,48,2048]{2,1,0:T(8,128)(2,1)}, u32[]{:S(2)}) copy-start(bf16[8,48,2048]{2,1,0:T(8,128)(2,1)} %get-tuple-element.26) | copy-start | bytes 4718596
  68.7 2.9 %copy-start.2 = (bf16[384,384]{1,0:T(8,128)(2,1)S(1)}, bf16[384,384]{1,0:T(8,128)(2,1)}, u32[]{:S(2)}) copy-start(bf16[384,384]{1,0:T(8,128)(2,1)} %get-tuple-element.25) | copy-start | bytes 884740
  71.5 2.7 %copy-start.5 = (bf16[128,512]{1,0:T(8,128)(2,1)S(1)}, bf16[128,512]{1,0:T(8,128)(2,1)}, u32[]{:S(2)}) copy-start(bf16[128,512]{1,0:T(8,128)(2,1)} %get-tuple-element.40) | copy-start | bytes 393220
  71.5 3.4 %copy-start.8 = (f32[2,128]{1,0:T(2,128)S(1)}, f32[2,128]{1,0:T(2,128)}, u32[]{:S(2)}) copy-start(f32[2,128]{1,0:T(2,128)} %get-tuple-element.21) | copy-start | bytes 3076
  71.5 3.9 %copy-start.3 = (f32[48,2048]{1,0:T(8,128)S(1)}, f32[48,2048]{1,0:T(8,128)}, u32[]{:S(2)}) copy-start(f32[48,2048]{1,0:T(8,128)} %get-tuple-element.45) | copy-start | bytes 1179652
  71.5 4.7 %copy-start.6 = (f32[2,2048]{1,0:T(2,128)S(1)}, f32[2,2048]{1,0:T(2,128)}, u32[]{:S(2)}) copy-start(f32[2,2048]{1,0:T(2,128)} %get-tuple-element.28) | copy-start | bytes 49156
  71.5 5.3 %copy-start.7 = (f32[1,384]{1,0:T(1,128)S(1)}, f32[1,384]{1,0:T(1,128)}, u32[]{:S(2)}) copy-start(f32[1,384]{1,0:T(1,128)} %get-tuple-element.47) | copy-start | bytes 4612
  71.5 5.8 %copy-start.9 = (f32[1,48]{1,0:T(1,128)S(1)}, f32[1,48]{1,0:T(1,128)}, u32[]{:S(2)}) copy-start(f32[1,48]{1,0:T(1,128)} %get-tuple-element.30) | copy-start | bytes 580
